TPU v7x, 32 devices: a whole 2x2x4 slice. The times are simulated.
32 devices in a mesh: sp: 8 (over z, x), tp: 4 (over y, core).
Axes of the slice: x: 2, y: 2, z: 4, core: 2. Of those that a mesh axis runs over, the one named last changes fastest.
Arguments:
- inputs: bfloat16 [3072, 2048], P('sp', 'tp'), may hold values from -6 to 6
- norm_gain: float32 [2048], replicated, may hold values from 0.1 to 1.9
- query_weight: bfloat16 [2048, 1024], P(None, 'tp')
- key_weight: bfloat16 [2048, 1024], P(None, 'tp'), may hold values from -0.15625 to 0.15625
- value_weight: bfloat16 [2048, 1024], P(None, 'tp'), may hold values from -0.125 to 0.125
- memory_query_weight: bfloat16 [2048, 1024], P(None, 'tp'), may hold values from -0.125 to 0.125
- memory_key_weight: bfloat16 [2048, 1024], P(None, 'tp'), may hold values from -0.125 to 0.125
- memory_value_weight: bfloat16 [2048, 1024], P(None, 'tp'), may hold values from -0.125 to 0.125
- input_gate_weight: bfloat16 [2048, 16], P(None, 'tp')
- forget_gate_weight: bfloat16 [2048, 16], P(None, 'tp'), may hold values from -0.3125 to 0.3125
- forget_bias: float32 [16], P('tp'), may hold values from 3 to 13
- decay_shift: float32 [3072, 16], P('sp', 'tp'), may hold values from -2 to 0, as said below
- lambdas: float32 [16], P('tp'), may hold values from 0.3 to 0.8
- head_gain: float32 [64], replicated, may hold values from 0.1 to 1.9
- out_weight_attention: bfloat16 [1024, 2048], P('tp'), may hold values from -0.125 to 0.125
- out_weight_memory: bfloat16 [1024, 2048], P('tp'), may hold values from -0.125 to 0.125
Outputs:
- combined: bfloat16 [3072, 2048], P('sp', 'tp')
Inputs may be any that keep to these rules, and one draw needn't show every extreme that they name: `decay_shift`: never positive.
All inputs are finite; a program needn't handle non-finite values.
Results may differ from a plain program's by a relative error of at most 0.018.
The roundings to bfloat16 on the way count: a program that leaves them out, or rounds other values in their place, can miss the bound.
Values may be sent and summed in bfloat16 or wider, within the bound.
A program may use at most 192 MiB of HBM per device.

v0:
```python
import jax
import jax.numpy as jnp
from jax import lax
from jax.sharding import PartitionSpec as P

HEAD = 64
DD = 32
BLOCK = 64
EPSILON = 1e-06
ROTARY_BASE = 10000.0
NEGATIVE = -1e30


def carried_in(part, axis, combine, identity):
    place = lax.axis_index(axis)
    gathered = jax.tree.map(lambda a: lax.all_gather(a, axis), part)
    state = jax.tree.map(lambda a, e: jnp.zeros_like(a) + jnp.asarray(e, a.dtype), part, identity)

    def one(hop, state):
        return combine(
            state, jax.tree.map(lambda a: lax.dynamic_index_in_dim(a, hop, 0, False), gathered)
        )

    return lax.fori_loop(0, place, one, state)


def rotate(halves, positions):
    middle = halves.shape[-1] // 2
    inverse = 1.0 / ROTARY_BASE ** (jnp.arange(middle, dtype=jnp.float32) / middle)
    angles = positions.astype(jnp.float32)[:, None] * inverse[None, :]
    cosine = jnp.cos(angles)[:, None, :]
    sine_part = jnp.sin(angles)[:, None, :]
    floats = halves.astype(jnp.float32)
    former = floats[..., :middle]
    latter = floats[..., middle:]
    turned = jnp.concatenate(
        [former * cosine - latter * sine_part, latter * cosine + former * sine_part], axis=-1
    )
    return turned.astype(jnp.bfloat16)


def advance_state(carried, block_entry):
    memory, normal, stable = carried
    block_memory, block_normal, block_max, block_decay = block_entry
    new_stable = jnp.maximum(block_decay + stable, block_max)
    former = jnp.exp(block_decay + stable - new_stable)
    latter = jnp.exp(block_max - new_stable)
    return (
        former[:, None, None] * memory + latter[:, None, None] * block_memory,
        former[:, None] * normal + latter[:, None] * block_normal,
        new_stable,
    )


def memory_blocks(queries, key_heads, values, gate_in, log_forget, entering):
    token_count, head_count, head_width = queries.shape
    block_count = token_count // BLOCK
    highest = lax.Precision.HIGHEST

    def blocked(flat_array):
        return (
            flat_array.astype(jnp.float32)
            .reshape(block_count, BLOCK, head_count, head_width)
            .transpose(2, 0, 1, 3)
        )

    query_blocks = blocked(queries)
    key_blocks = blocked(key_heads) * head_width ** (-0.5)
    value_blocks = blocked(values)
    gate_blocks = gate_in.reshape(block_count, BLOCK, head_count).transpose(2, 0, 1)
    cumulative = jnp.cumsum(
        log_forget.reshape(block_count, BLOCK, head_count).transpose(2, 0, 1), axis=-1
    )
    block_ends = cumulative[..., -1]
    toward_end = block_ends[..., None] - cumulative + gate_blocks
    local_max = jnp.max(toward_end, axis=-1)
    end_weights = jnp.exp(toward_end - local_max[..., None])
    local_memory = jnp.einsum(
        "hcl,hclv,hclk->chvk", end_weights, value_blocks, key_blocks, precision=highest
    )
    local_normal = jnp.einsum("hcl,hclk->chk", end_weights, key_blocks, precision=highest)

    def scan_step(carried, block_entry):
        return (advance_state(carried, block_entry), carried)

    entries = (local_memory, local_normal, local_max.T, block_ends.T)
    unused, (memory_in, normal_in, stable_in) = lax.scan(scan_step, entering, entries)
    lower_mask = jnp.tril(jnp.ones((BLOCK, BLOCK), dtype=bool))
    decays = jnp.where(
        lower_mask,
        cumulative[..., :, None] - cumulative[..., None, :] + gate_blocks[..., None, :],
        NEGATIVE,
    )
    carried_log = cumulative + stable_in.T[..., None]
    row_max = jnp.maximum(carried_log, jnp.max(decays, axis=-1))
    within = jnp.where(lower_mask, jnp.exp(decays - row_max[..., None]), 0.0)
    outside = jnp.exp(carried_log - row_max)
    scores = within * jnp.einsum("hctd,hcsd->hcts", query_blocks, key_blocks, precision=highest)
    numerator = outside[..., None] * jnp.einsum(
        "chvk,hctk->hctv", memory_in, query_blocks, precision=highest
    )
    numerator = numerator + jnp.einsum("hcts,hcsv->hctv", scores, value_blocks, precision=highest)
    denominator = outside * jnp.einsum(
        "chk,hctk->hct", normal_in, query_blocks, precision=highest
    ) + jnp.sum(scores, axis=-1)
    result = numerator / jnp.maximum(jnp.abs(denominator), 1.0)[..., None]
    return (
        result.transpose(1, 2, 0, 3)
        .reshape(token_count, head_count * head_width)
        .astype(jnp.bfloat16)
    )


def combine_states(earlier, later_part):
    memory, normal, stable, decay_sum = earlier
    later_memory, later_normal, later_stable, later_decay = later_part
    new_stable = jnp.maximum(later_decay + stable, later_stable)
    former = jnp.exp(later_decay + stable - new_stable)
    latter = jnp.exp(later_stable - new_stable)
    return (
        former[:, None, None] * memory + latter[:, None, None] * later_memory,
        former[:, None] * normal + latter[:, None] * later_normal,
        new_stable,
        decay_sum + later_decay,
    )


def summarize(key_heads, values, gate_in, log_forget):
    head_width = key_heads.shape[-1]
    highest = lax.Precision.HIGHEST
    key_floats = key_heads.astype(jnp.float32) * head_width ** (-0.5)
    cumulative = jnp.cumsum(log_forget, axis=0)
    span_decay = cumulative[-1]
    toward_end = span_decay[None, :] - cumulative + gate_in
    span_max = jnp.max(toward_end, axis=0)
    end_weights = jnp.exp(toward_end - span_max[None, :])
    memory = jnp.einsum(
        "rh,rhv,rhk->hvk", end_weights, values.astype(jnp.float32), key_floats, precision=highest
    )
    normal = jnp.einsum("rh,rhk->hk", end_weights, key_floats, precision=highest)
    return (memory, normal, span_max, span_decay)


def attend(carried, arriving, query_first, query_second, query_positions):
    key_first = arriving[..., :DD]
    key_second = arriving[..., DD : 2 * DD]
    value_part = arriving[..., 2 * DD :]
    key_positions = jnp.arange(arriving.shape[0], dtype=jnp.int32)
    visible = (key_positions[None, :] <= query_positions[:, None]) & (key_positions[None, :] >= 0)
    score_scale = DD ** (-0.5)
    results = []
    for side_index, (query_side, key_side) in enumerate(
        ((query_first, key_first), (query_second, key_second))
    ):
        row_max, totals, accumulated = carried[3 * side_index : 3 * side_index + 3]
        scores = (
            jnp.einsum("qhd,khd->hqk", query_side, key_side, preferred_element_type=jnp.float32)
            * score_scale
        )
        scores = jnp.where(visible[None], scores, NEGATIVE)
        new_max = jnp.maximum(row_max, jnp.max(scores, axis=2))
        weights = jnp.where(visible[None], jnp.exp(scores - new_max[..., None]), 0.0)
        totals = jnp.sum(weights, axis=2)
        accumulated = jnp.einsum(
            "hqk,khd->hqd",
            weights.astype(jnp.bfloat16),
            value_part,
            preferred_element_type=jnp.float32,
        )
        results.extend([new_max, totals, accumulated])
    return tuple(results)


def per_device(
    inputs,
    norm_gain,
    query_weight,
    key_weight,
    value_weight,
    memory_query_weight,
    memory_key_weight,
    memory_value_weight,
    input_gate_weight,
    forget_gate_weight,
    forget_bias,
    decay_shift,
    lambdas,
    head_gain,
    out_weight_attention,
    out_weight_memory,
):
    row_count = inputs.shape[0]
    weights = (
        query_weight,
        key_weight,
        value_weight,
        memory_query_weight,
        memory_key_weight,
        memory_value_weight,
        input_gate_weight,
        forget_gate_weight,
    )
    floats = lax.all_gather(inputs, "tp", axis=1, tiled=True).astype(jnp.float32)
    scaled = (floats * norm_gain[None, :]).astype(jnp.bfloat16)
    running_sums = tuple(
        (jnp.dot(scaled, weight, preferred_element_type=jnp.float32) for weight in weights)
    )
    running_sums, squares = (running_sums, jnp.sum(floats * floats, axis=1))
    inverse_rms = lax.rsqrt(squares / norm_gain.shape[0] + EPSILON)[:, None]
    projected = [running * inverse_rms for running in running_sums]

    def split_heads(flat_values):
        return flat_values.astype(jnp.bfloat16).reshape(row_count, -1, HEAD)

    queries = split_heads(projected[0])
    key_heads = split_heads(projected[1])
    values = split_heads(projected[2])
    offset = lax.axis_index("sp") * row_count
    positions = offset + jnp.arange(row_count, dtype=jnp.int32)
    query_first = rotate(queries[..., :DD], positions)
    query_second = rotate(queries[..., DD:], positions)
    packed = jnp.concatenate(
        [rotate(key_heads[..., :DD], positions), rotate(key_heads[..., DD:], positions), values],
        axis=-1,
    )
    head_count = queries.shape[1]
    empty_max = jnp.full((head_count, row_count), NEGATIVE, jnp.float32)
    empty_total = jnp.zeros((head_count, row_count), jnp.float32)
    empty_sums = jnp.zeros((head_count, row_count, HEAD), jnp.float32)
    starting = (empty_max, empty_total, empty_sums, empty_max, empty_total, empty_sums)
    gathered = attend(
        starting,
        lax.all_gather(packed, "sp", axis=0, tiled=True),
        query_first,
        query_second,
        positions,
    )
    first_max, first_total, first_sums, second_max, second_total, second_sums = gathered
    stacked = first_sums / first_total[..., None] - lambdas[:, None, None] * (
        second_sums / second_total[..., None]
    )
    stacked = stacked.transpose(1, 0, 2)
    norm_scale = lax.rsqrt(jnp.mean(stacked * stacked, axis=-1, keepdims=True) + EPSILON)
    attended = (stacked * norm_scale * head_gain).astype(jnp.bfloat16).reshape(row_count, -1)
    gate_in = projected[6]
    log_forget = jax.nn.log_sigmoid(projected[7] + forget_bias[None, :]) + decay_shift
    memory_queries = split_heads(projected[3])
    memory_keys = split_heads(projected[4])
    memory_values = split_heads(projected[5])
    summary = summarize(memory_keys, memory_values, gate_in, log_forget)
    memory_heads = gate_in.shape[1]
    identity = (
        jnp.zeros((memory_heads, HEAD, HEAD), jnp.float32),
        jnp.zeros((memory_heads, HEAD), jnp.float32),
        jnp.full((memory_heads,), NEGATIVE, jnp.float32),
        jnp.zeros((memory_heads,), jnp.float32),
    )
    prefix = carried_in(summary, "sp", combine_states, identity)
    start_state = (
        jnp.zeros((memory_heads, HEAD, HEAD), jnp.float32),
        jnp.zeros((memory_heads, HEAD), jnp.float32),
        jnp.zeros((memory_heads,), jnp.float32),
        jnp.zeros((memory_heads,), jnp.float32),
    )
    entering = combine_states(start_state, prefix)[:3]
    memory = memory_blocks(
        memory_queries, memory_keys, memory_values, gate_in, log_forget, entering
    )
    partial_term = jnp.dot(attended, out_weight_attention, preferred_element_type=jnp.float32)
    partial_term = partial_term + jnp.dot(
        memory, out_weight_memory, preferred_element_type=jnp.float32
    )
    return lax.psum_scatter(
        partial_term.astype(jnp.bfloat16), "tp", scatter_dimension=1, tiled=True
    )


def solution(mesh):
    in_specs = (
        P("sp", "tp"),
        P(),
        P(None, "tp"),
        P(None, "tp"),
        P(None, "tp"),
        P(None, "tp"),
        P(None, "tp"),
        P(None, "tp"),
        P(None, "tp"),
        P(None, "tp"),
        P("tp"),
        P("sp", "tp"),
        P("tp"),
        P(),
        P("tp", None),
        P("tp", None),
    )
    out_specs = P("sp", "tp")
    return jax.shard_map(
        per_device, mesh=mesh, in_specs=in_specs, out_specs=out_specs, check_vma=False
    )
```

profile of v0, /device:TPU:0, one launch (start us, length us, event | category | flops | bytes accessed | tf_op | source)
XLA Modules:
  0.0 310.0 jit_solution(3127829194106254127)
XLA Ops:
  7.4 1.2 dynamic-slice
  10.2 21.1 %all-gather.8.cloned.1.call-done = bf16[384,2048]{1,0:T(8,128)(2,1)} async-done(((bf16[384,512]{1,0:T(8,128)(2,1)}), bf16[384,2048]{1,0:T(8,128)(2,1)}) %all-gather.8.cloned.1.call-update) | async-done | bytes 1572880 | tf_op jit(solution)/shard_map/all_gather | solution.py:203
  31.3 1.8 fusion.26
  33.2 1.9 fusion.113
  35.2 1.2 reduce-window.6
  37.0 2.0 fusion.128
  39.5 21.3 %all-reduce = f32[32]{0:T(128)S(1)} all-reduce(f32[32]{0:T(128)S(1)} %dynamic-update-slice), channel_id=2, replica_groups=mesh['sp'=8,'tp'=4] {'sp'}, use_global_device_ids=true, to_apply=%add | all-reduce | flops 32 | bytes 256
  60.9 16.7 %all-gather.3 = f32[8,1,4]{2,1,0:T(1,128)} all-gather(f32[1,1,4]{2,1,0:T(1,128)S(1)} %bitcast.225), channel_id=1, replica_groups=mesh['sp'=8,'tp'=4] {'sp'}, dimensions={0}, use_global_device_ids=true | all-gather | bytes 144 | tf_op jit(solution)/shard_map/all_gather | solution.py:16
  77.6 0.9 reduce_window_sum.28
  79.6 2.5 fusion.46
  82.5 0.8 copy.55
  83.3 2.5 fusion.49
  85.8 0.9 copy.57
  86.7 1.2 fusion.84
  88.5 26.1 %all-gather.4 = f32[8,4,64]{2,1,0:T(4,128)S(1)} all-gather(f32[1,4,64]{2,1,0:T(4,128)S(1)} %bitcast.221), channel_id=4, replica_groups=mesh['sp'=8,'tp'=4] {'sp'}, dimensions={0}, use_global_device_ids=true | all-gather | bytes 9216 | tf_op jit(solution)/shard_map/all_gather | solution.py:16
  114.6 2.5 fusion.44
  117.2 0.8 fusion.45
  118.1 0.7 copy-done.8
  118.9 1.3 mul.423
  120.2 0.8 fusion.81
  121.0 1.4 convert_multiply_fusion.2
  122.4 2.3 fusion.78
  124.7 36.9 %all-gather.1 = f32[32,64,64]{2,1,0:T(8,128)} all-gather(f32[4,64,64]{2,1,0:T(8,128)S(1)} %copy-done.7), channel_id=3, replica_groups=mesh['sp'=8,'tp'=4] {'sp'}, dimensions={0}, use_global_device_ids=true | all-gather | bytes 589824 | tf_op jit(solution)/shard_map/all_gather | solution.py:16
  162.0 18.5 %while.37 = (s32[]{:T(128)}, f32[4,64,64]{2,1,0:T(8,128)S(1)}, f32[4,64]{1,0:T(4,128)S(1)}, f32[4]{0:T(128)S(1)}, f32[6,4,64,64]{3,2,0,1:T(8,128)}, /*index=5*/f...) while((s32[]{:T(128)}, f32[4,64,64]{2,1,0:T(8,128)S(1)}, ...), condition=%wide.region_14.15_spmd, body=%wide.region_13.14_spmd.sunk | while | flops 49938 | bytes 399745 | solution.py:87
  162.0 0.7 subtract_exponential_fusion.13
  164.1 1.0 fusion.159
  167.2 1.0 fusion.159
  170.3 1.0 fusion.159
  171.3 0.7 subtract_exponential_fusion.13
  173.3 1.0 fusion.159
  176.4 1.0 fusion.159
  179.5 1.0 fusion.159
  180.5 3.1 %fusion.50 = bf16[384,256]{0,1:T(8,128)(2,1)} fusion(bf16[2048,256]{1,0:T(8,128)(2,1)} %param.25, bf16[384,2048]{1,0:T(8,128)(2,1)} %all-gather.8.cloned.1.call-done, f32[2048]{0:T(1024)S(1)} %copy-done.22, f32[384]{0:T(512)S(1)} %copy-done.11), kind=kOutput, calls=%fused_computation.71 | convolution fusion | flops 405209088 | bytes 2827776 | tf_op jit(solution)/shard_map/dot_general | solution.py:206
  183.6 1.8 copy.64
  185.4 1.9 reshape.199
  187.3 1.9 copy.80
  190.1 1.4 fusion.109
  191.5 1.7 fusion.132
  193.3 0.8 convolution_bitcast_fusion
  194.2 0.9 fusion.32
  195.7 2.5 fusion.43
  198.3 10.2 %fusion.75 = f32[4,384,3072]{2,1,0:T(8,128)} fusion(bf16[3072,4,128]{0,2,1:T(8,128)(2,1)} %all-gather.10.cloned.1.call-done, bf16[384,4,16]{0,2,1:T(8,128)(2,1)S(1)} %get-tuple-element.253, bf16[384,4,16]{0,2,1:T(8,128)(2,1)S(1)} %get-tuple-element.254), kind=kOutput, calls=%fused_computation.82 | convolution fusion | flops 302186496 | bytes 19759104 | tf_op jit(solution)/shard_map/qhd,khd->hqk/dot_general | solution.py:157
  208.5 17.6 %fusion.14 = (f32[4,384]{1,0:T(4,128)S(1)}, f32[4,384]{1,0:T(4,128)S(1)}, f32[4,384,3072]{2,1,0:T(8,128)}) fusion(pred[384,3072]{1,0:T(8,128)(4,1)S(1)} %iota_compare_fusion, f32[4,384,3072]{2,1,0:T(8,128)} %fusion.75, bf16[3072,4,128]{0,2,1:T(8,128)(2,1)} %all-gather.10.cloned.1.call-done, bf16[384,4,16]{0,2,1:T(8,128)(2,1)S(1)} %get-tuple-element.246, ...), kind=kOutput, calls=%fused_computation.32 | convolution fusion | flops 330494976 | bytes 39825408 | tf_op jit(solution)/shard_map/qhd,khd->hqk/dot_general | solution.py:157
  226.1 17.6 %fusion.17 = (f32[4,384]{1,0:T(4,128)S(1)}, f32[4,384]{1,0:T(4,128)S(1)}) fusion(f32[4,384,3072]{2,1,0:T(8,128)} %get-tuple-element.257, f32[4,384]{1,0:T(4,128)S(1)} %get-tuple-element.264, pred[384,3072]{1,0:T(8,128)(4,1)} %copy-done.2, f32[4,384]{1,0:T(4,128)S(1)} %get-tuple-element.265, f32[4,384,3072]{2,1,0:T(8,128)} %fusion.75), kind=kLoop, calls=%fused_computation.35 | loop fusion | flops 47182848 | bytes 38952960 | tf_op jit(solution)/shard_map/reduce_sum | solution.py:163
  244.0 8.0 %fusion.68 = f32[384,4,64]{0,2,1:T(8,128)S(1)} fusion(bf16[3072,4,128]{0,2,1:T(8,128)(2,1)} %all-gather.10.cloned.1.call-done, f32[4,384,3072]{2,1,0:T(8,128)S(1)} %copy-done.1, f32[4,384]{1,0:T(4,128)S(1)} %get-tuple-element.265, pred[384,3072]{1,0:T(8,128)(4,1)} %copy-done.2, f32[384,4]{0,1:T(4,128)S(1)} %bitcast.224), kind=kOutput, calls=%fused_computation.79 | convolution fusion | flops 627671040 | bytes 22032384 | tf_op jit(solution)/shard_map/hqk,khd->hqd/dot_general | solution.py:164
  252.0 9.9 %multiply_reduce_fusion = (f32[384,4]{0,1:T(4,128)S(1)}, f32[384,4,64]{0,2,1:T(8,128)S(1)}) fusion(f32[384,4,64]{0,2,1:T(8,128)S(1)} %fusion.68, f32[384,4]{0,1:T(4,128)S(1)} %bitcast.223, bf16[3072,4,128]{0,2,1:T(8,128)(2,1)} %all-gather.10.cloned.1.call-done, f32[4,384,3072]{2,1,0:T(8,128)} %get-tuple-element.257, f32[4,384]{1,0:T(4,128)S(1)} %get-tuple-element.264, ...), kind=kOutput, calls=%fused_computation.97 | convolution fusion | flops 628062720 | bytes 22431760 | tf_op jit(solution)/shard_map/hqk,khd->hqd/dot_general | solution.py:164
  263.1 1.8 add_convert_fusion
  264.9 38.5 %reduce-scatter.2.cloned.1.call-done = bf16[384,512]{1,0:T(8,128)(2,1)} async-done(((bf16[384,2048]{1,0:T(8,128)(2,1)}), bf16[384,512]{1,0:T(8,128)(2,1)}) %reduce-scatter.2.cloned.1.call-update) | async-done | bytes 393232 | tf_op jit(solution)/shard_map/reduce_scatter | solution.py:273
  (152 shorter events, 19.5 us)
Async XLA Ops:
  6.5 255.5 %copy-start = (bf16[256,2048]{1,0:T(8,128)(2,1)S(1)}, bf16[256,2048]{1,0:T(8,128)(2,1)}, u32[]{:S(2)}) copy-start(bf16[256,2048]{1,0:T(8,128)(2,1)} %param.34) | copy-start | bytes 3145732
  6.5 26.6 %copy-start.19 = (f32[2048]{0:T(1024)S(1)}, f32[2048]{0:T(1024)}, u32[]{:S(2)}) copy-start(f32[2048]{0:T(1024)} %param.21) | copy-start | bytes 24580
  6.5 26.6 %copy-start.24 = (f32[384,4]{0,1:T(4,128)S(1)}, f32[384,4]{0,1:T(4,128)}, u32[]{:S(2)}) copy-start(f32[384,4]{0,1:T(4,128)} %param.31) | copy-start | bytes 18436
  6.5 26.6 %copy-start.25 = (f32[4]{0:T(128)S(1)}, f32[4]{0:T(128)}, u32[]{:S(2)}) copy-start(f32[4]{0:T(128)} %param.30) | copy-start | bytes 52
  6.5 26.6 %copy-start.16 = (bf16[2048,4]{0,1:T(4,128)(2,1)S(1)}, bf16[2048,4]{0,1:T(4,128)(2,1)}, u32[]{:S(2)}) copy-start(bf16[2048,4]{0,1:T(4,128)(2,1)} %param.29) | copy-start | bytes 49156
  6.5 30.5 %copy-start.17 = (bf16[2048,4]{0,1:T(4,128)(2,1)S(1)}, bf16[2048,4]{0,1:T(4,128)(2,1)}, u32[]{:S(2)}) copy-start(bf16[2048,4]{0,1:T(4,128)(2,1)} %param.28) | copy-start | bytes 49156
  6.6 24.8 %all-gather.8.cloned.1.call-start = ((), (), s32[]{:S(2)}) async-start(), calls=%async_computation.1 | async-start | bytes 1966080 | tf_op jit(solution)/shard_map/all_gather | solution.py:203
  7.3 191.0 %all-gather.10.cloned.1.call-start = ((), (), s32[]{:S(2)}) async-start(), calls=%async_computation.2 | async-start | bytes 3538944 | tf_op jit(solution)/shard_map/all_gather | solution.py:233
  10.2 198.3 %copy-start.2 = (pred[384,3072]{1,0:T(8,128)(4,1)}, pred[384,3072]{1,0:T(8,128)(4,1)S(1)}, u32[]{:S(2)}) copy-start(pred[384,3072]{1,0:T(8,128)(4,1)S(1)} %iota_compare_fusion) | copy-start | bytes 3538948
  33.2 84.0 %copy-start.10 = (f32[384]{0:T(512)}, f32[384]{0:T(512)S(1)}, u32[]{:S(2)}) copy-start(f32[384]{0:T(512)S(1)} %add_rsqrt_fusion.1) | copy-start | bytes 4612
  82.5 38.5 %copy-start.3 = (bf16[6,64,4,64]{3,2,1,0:T(4,128)(2,1)}, bf16[6,64,4,64]{3,2,1,0:T(4,128)(2,1)S(1)}, u32[]{:S(2)}) copy-start(bf16[6,64,4,64]{3,2,1,0:T(4,128)(2,1)S(1)} %reshape.198) | copy-start | bytes 589828
  82.5 32.1 %copy-start.20 = (f32[2048]{0:T(1024)S(1)}, f32[2048]{0:T(1024)}, u32[]{:S(2)}) copy-start(f32[2048]{0:T(1024)} %param.21) | copy-start | bytes 24580
  86.7 30.5 %copy-start.5 = (bf16[384,2048]{1,0:T(8,128)(2,1)S(1)}, bf16[384,2048]{1,0:T(8,128)(2,1)}, u32[]{:S(2)}) copy-start(bf16[384,2048]{1,0:T(8,128)(2,1)} %all-gather.8.cloned.1.call-done) | copy-start | bytes 4718596
  86.7 30.5 %copy-start.14 = (bf16[2048,256]{1,0:T(8,128)(2,1)S(1)}, bf16[2048,256]{1,0:T(8,128)(2,1)}, u32[]{:S(2)}) copy-start(bf16[2048,256]{1,0:T(8,128)(2,1)} %param.24) | copy-start | bytes 3145732
  86.7 30.5 %copy-start.21 = (f32[2048]{0:T(1024)S(1)}, f32[2048]{0:T(1024)}, u32[]{:S(2)}) copy-start(f32[2048]{0:T(1024)} %param.21) | copy-start | bytes 24580
  118.0 0.7 copy-start.8
  118.8 184.6 %reduce-scatter.2.cloned.1.call-start = ((), (), s32[]{:S(2)}) async-start(), calls=%async_computation.3 | async-start | bytes 1966080 | tf_op jit(solution)/shard_map/reduce_scatter | solution.py:273
  120.2 4.5 %copy-start.7 = (f32[4,64,64]{2,1,0:T(8,128)S(1)}, f32[4,64,64]{2,1,0:T(8,128)}, u32[]{:S(2)}) copy-start(f32[4,64,64]{2,1,0:T(8,128)} %fusion.84) | copy-start | bytes 196612
  161.6 18.9 %copy-start.11 = (f32[384]{0:T(512)S(1)}, f32[384]{0:T(512)}, u32[]{:S(2)}) copy-start(f32[384]{0:T(512)} %copy-done.10) | copy-start | bytes 4612
  161.6 18.9 %copy-start.22 = (f32[2048]{0:T(1024)S(1)}, f32[2048]{0:T(1024)}, u32[]{:S(2)}) copy-start(f32[2048]{0:T(1024)} %param.21) | copy-start | bytes 24580
  180.5 9.6 %copy-start.18 = (f32[6,4,64]{2,1,0:T(4,128)S(1)}, f32[6,4,64]{2,1,0:T(4,128)}, u32[]{:S(2)}) copy-start(f32[6,4,64]{2,1,0:T(4,128)} %get-tuple-element.126) | copy-start | bytes 18436
  183.6 9.7 %copy-start.4 = (bf16[6,64,4,64]{3,2,1,0:T(4,128)(2,1)S(1)}, bf16[6,64,4,64]{3,2,1,0:T(4,128)(2,1)}, u32[]{:S(2)}) copy-start(bf16[6,64,4,64]{3,2,1,0:T(4,128)(2,1)} %copy-done.3) | copy-start | bytes 589828
  189.5 4.7 %copy-start.9 = (bf16[4,6,64,64]{2,3,1,0:T(8,128)(2,1)S(1)}, bf16[4,6,64,64]{2,3,1,0:T(8,128)(2,1)}, u32[]{:S(2)}) copy-start(bf16[4,6,64,64]{2,3,1,0:T(8,128)(2,1)} %copy.80) | copy-start | bytes 589828
  189.5 4.7 %copy-start.15 = (f32[6,4,64,64]{3,2,0,1:T(8,128)S(1)}, f32[6,4,64,64]{3,2,0,1:T(8,128)}, u32[]{:S(2)}) copy-start(f32[6,4,64,64]{3,2,0,1:T(8,128)} %get-tuple-element.125) | copy-start | bytes 1179652
  193.3 2.3 copy-start.12
  193.3 2.3 copy-start.23
  226.1 17.9 %copy-start.1 = (f32[4,384,3072]{2,1,0:T(8,128)S(1)}, f32[4,384,3072]{2,1,0:T(8,128)}, u32[]{:S(2)}) copy-start(f32[4,384,3072]{2,1,0:T(8,128)} %fusion.75) | copy-start | bytes 56623108
  244.0 8.0 %copy-start.26 = (f32[4]{0:T(128)S(1)}, f32[4]{0:T(128)}, u32[]{:S(2)}) copy-start(f32[4]{0:T(128)} %param.32) | copy-start | bytes 52
  252.0 9.9 %copy-start.13 = (f32[64]{0:T(128)S(1)}, f32[64]{0:T(128)}, u32[]{:S(2)}) copy-start(f32[64]{0:T(128)} %param.33) | copy-start | bytes 772
  261.9 1.2 copy-start.6
Sparse Core Ops, SparseCore 0:
  8.9 22.3 all-gather.7
  118.9 66.6 all-gather.9
  265.0 38.3 reduce-scatter.1
where the time goes:
time: 311 us; the launch traced here: 310 us
  blocking collectives  101 us (32%)
  matrix products  75.5 us (24%)
  waiting for transfers between devices  60.4 us (19%)
  other arithmetic  36.2 us (12%)
  local copies, waits for them, and re-layouts  22.1 us (7%)
  between operations  14.4 us (5%)
    all_gather x3, blocking collectives, carried_in(): gathered = jax.tree.map(lambda a: lax.all_gather(a, axis), part)  79.7 us
    reduce_scatter x1, waiting for transfers between devices, per_device(): lax.psum_scatter(partial_term.astype(jnp.bfloat16), 'tp', scatter_dimensi...  38.5 us
    dot_general x2, matrix products, attend(): jnp.einsum('qhd,khd->hqk', query_side, key_side, preferred_element_type=j...  27.8 us
    unnamed x1, blocking collectives  21.3 us
    all_gather x1, waiting for transfers between devices, per_device(): lax.all_gather(inputs, 'tp', axis=1, tiled=True).astype(jnp.float32)  21.1 us
    dot_general x2, matrix products, attend(): jnp.einsum('hqk,khd->hqd', weights.astype(jnp.bfloat16), value_part, pref...  17.9 us
    dot_general x8, matrix products, per_device(): jnp.dot(scaled, weight, preferred_element_type=jnp.float32)  17.7 us
    reduce_sum x1, other arithmetic, attend(): totals = jnp.sum(weights, axis=2)  17.6 us
  transfers between devices with their start and end apart: 3, of which 2 were waited for; matrix products, arithmetic and copies ran while one was open for 14% of the time, Pallas kernels for 0%

commit v1 on v0

--- a/solution.py
+++ b/solution.py
@@ -2,6 +2,7 @@
 import jax.numpy as jnp
 from jax import lax
 from jax.sharding import PartitionSpec as P
+from jax.lax import all_to_all, axis_size
 
 HEAD = 64
 DD = 32
@@ -200,7 +201,12 @@
         input_gate_weight,
         forget_gate_weight,
     )
-    floats = lax.all_gather(inputs, "tp", axis=1, tiled=True).astype(jnp.float32)
+
+    def view_sites(block_in):
+        row_out = jnp.concatenate([block_in for _ in range(axis_size("tp"))], 1)
+        return all_to_all(row_out, axis_name="tp", split_axis=1, concat_axis=1, tiled=True)
+
+    floats = view_sites(inputs).astype(jnp.float32)
     scaled = (floats * norm_gain[None, :]).astype(jnp.bfloat16)
     running_sums = tuple(
         (jnp.dot(scaled, weight, preferred_element_type=jnp.float32) for weight in weights)

time: 311 us -> 368 us (1.18)
  local copies, waits for them, and re-layouts: 22.1 us -> 43.5 us
  other arithmetic: 36.2 us -> 56.4 us
  waiting for transfers between devices: 60.4 us -> 70.7 us
  matrix products: 75.5 us -> 70.9 us
  starting transfers between devices: 0.12 us -> 4.42 us
    all_gather x1 -> x0, waiting for transfers between devices: 21.1 us -> none  [per_device(): lax.all_gather(inputs, 'tp', axis=1, tiled=True).astype(jnp.float32)]
    all_to_all x0 -> x1, waiting for transfers between devices: none -> 16.9 us  [view_sites(): all_to_all(row_out, axis_name='tp', split_axis=1, concat_axis=1, tiled=True)]
    reduce_scatter x1, waiting for transfers between devices: 38.5 us -> 53.7 us  [per_device(): lax.psum_scatter(partial_term.astype(jnp.bfloat16), 'tp', scatter_dimensi...]
    dynamic_update_slice x18, local copies, waits for them, and re-layouts: 7.69 us -> 19.3 us  [memory_blocks(): lax.scan(scan_step, entering, entries)]
    add x6, other arithmetic: 0.47 us -> 8.04 us  [advance_state(): former[:, None] * normal + latter[:, None] * block_normal]
    dot_general x8, matrix products: 17.7 us -> 11.7 us  [per_device(): jnp.dot(scaled, weight, preferred_element_type=jnp.float32)]
    all_to_all x0 -> x1, starting transfers between devices: none -> 4.34 us  [view_sites(): all_to_all(row_out, axis_name='tp', split_axis=1, concat_axis=1, tiled=True)]
    exp x6, other arithmetic: 0.06 us -> 4.14 us  [advance_state(): latter = jnp.exp(block_max - new_stable)]
  transfers between devices with their start and end apart: 3 -> 3, of which waited for: 2 -> 2; matrix products, arithmetic and copies ran while one was open for 14% -> 21% of each run, Pallas kernels for 0% -> 0%
where the time goes in v1:
time: 368 us; the launch traced here: 365 us
  blocking collectives  104 us (28%)
  matrix products  70.9 us (19%)
  waiting for transfers between devices  70.7 us (19%)
  other arithmetic  56.4 us (15%)
  local copies, waits for them, and re-layouts  43.5 us (12%)
  between operations  14.8 us (4%)
  starting transfers between devices  4.42 us (1%)
    all_gather x3, blocking collectives, carried_in(): gathered = jax.tree.map(lambda a: lax.all_gather(a, axis), part)  81.8 us
    reduce_scatter x1, waiting for transfers between devices, per_device(): lax.psum_scatter(partial_term.astype(jnp.bfloat16), 'tp', scatter_dimensi...  53.7 us
    dot_general x2, matrix products, attend(): jnp.einsum('qhd,khd->hqk', query_side, key_side, preferred_element_type=j...  27.9 us
    unnamed x1, blocking collectives  22.4 us
    dynamic_update_slice x18, local copies, waits for them, and re-layouts, memory_blocks(): lax.scan(scan_step, entering, entries)  19.3 us
    dot_general x2, matrix products, attend(): jnp.einsum('hqk,khd->hqd', weights.astype(jnp.bfloat16), value_part, pref...  17.9 us
    reduce_sum x1, other arithmetic, attend(): totals = jnp.sum(weights, axis=2)  17.6 us
    all_to_all x1, waiting for transfers between devices, view_sites(): all_to_all(row_out, axis_name='tp', split_axis=1, concat_axis=1, tiled=True)  16.9 us
  transfers between devices with their start and end apart: 3, of which 2 were waited for; matrix products, arithmetic and copies ran while one was open for 21% of the time, Pallas kernels for 0%

profile of v1, /device:TPU:0, one launch (start us, length us, event | category | flops | bytes accessed | tf_op | source)
XLA Modules:
  0.0 365.0 jit_solution(14279131620874310758)
XLA Ops:
  6.5 1.3 copy.73
  8.0 1.6 copy.77
  9.6 4.3 %all-to-all-start = ((bf16[384,4,512]{2,0,1:T(8,128)(2,1)}), bf16[384,4,512]{2,0,1:T(8,128)(2,1)}, u32[]{:S(2)}, u32[]{:S(2)}) async-start(bf16[384,4,512]{2,0,1:T(8,128)(2,1)} %copy.77), calls=%async_computation | async-start | bytes 3145728 | tf_op jit(solution)/shard_map/all_to_all | solution.py:207
  16.2 1.7 iota_compare_fusion
  17.9 16.9 %all-to-all-done = bf16[384,4,512]{2,0,1:T(8,128)(2,1)} async-done(((bf16[384,4,512]{2,0,1:T(8,128)(2,1)}), bf16[384,4,512]{2,0,1:T(8,128)(2,1)}, u32[]{:S(2)}, u32[]{:S(2)}) %all-to-all-start) | async-done | bytes 1572896 | tf_op jit(solution)/shard_map/all_to_all | solution.py:207
  34.8 1.9 copy.78
  38.3 1.7 fusion.25
  43.2 22.4 %all-reduce = f32[32]{0:T(128)S(1)} all-reduce(f32[32]{0:T(128)S(1)} %dynamic-update-slice), channel_id=2, replica_groups=mesh['sp'=8,'tp'=4] {'sp'}, use_global_device_ids=true, to_apply=%add | all-reduce | flops 32 | bytes 256
  66.3 16.9 %all-gather.3 = f32[8,1,4]{2,1,0:T(1,128)} all-gather(f32[1,1,4]{2,1,0:T(1,128)S(1)} %bitcast.236), channel_id=1, replica_groups=mesh['sp'=8,'tp'=4] {'sp'}, dimensions={0}, use_global_device_ids=true | all-gather | bytes 144 | tf_op jit(solution)/shard_map/all_gather | solution.py:17
  85.8 2.0 fusion.45
  89.7 2.1 fusion.43
  91.8 1.4 fusion.44
  96.7 26.9 %all-gather.4 = f32[8,4,64]{2,1,0:T(4,128)} all-gather(f32[1,4,64]{2,1,0:T(4,128)S(1)} %bitcast.235), channel_id=4, replica_groups=mesh['sp'=8,'tp'=4] {'sp'}, dimensions={0}, use_global_device_ids=true | all-gather | bytes 9216 | tf_op jit(solution)/shard_map/all_gather | solution.py:17
  125.6 1.3 mul.424
  126.9 2.1 fusion.80
  129.0 1.6 convert_multiply_fusion
  130.6 2.4 fusion.77
  133.0 38.1 %all-gather.1 = f32[32,64,64]{2,1,0:T(8,128)} all-gather(f32[4,64,64]{2,1,0:T(8,128)S(1)} %copy-done.11), channel_id=3, replica_groups=mesh['sp'=8,'tp'=4] {'sp'}, dimensions={0}, use_global_device_ids=true | all-gather | bytes 589824 | tf_op jit(solution)/shard_map/all_gather | solution.py:17
  173.9 1.3 multiply_add_fusion.1
  176.2 44.6 %while.37 = (s32[]{:T(128)}, f32[4,64,64]{2,1,0:T(8,128)S(1)}, f32[4,64]{1,0:T(4,128)}, f32[4]{0:T(128)}, f32[6,4,64,64]{3,2,0,1:T(8,128)}, /*index=5*/f32[6,4,6...) while((s32[]{:T(128)}, f32[4,64,64]{2,1,0:T(8,128)S(1)}, ...), condition=%wide.region_14.15_spmd, body=%wide.region_13.14_spmd.sunk | while | flops 49938 | bytes 400769 | solution.py:88
  176.2 1.3 dynamic_update_slice.19
  180.6 1.3 fusion.157
  183.7 1.3 dynamic_update_slice.19
  188.1 1.3 fusion.157
  191.1 1.3 dynamic_update_slice.19
  195.5 1.3 fusion.157
  198.5 1.3 dynamic_update_slice.19
  201.7 1.3 bitcast_dynamic-update-slice_fusion.5
  203.0 1.3 fusion.157
  206.0 1.3 dynamic_update_slice.19
  209.1 1.3 bitcast_dynamic-update-slice_fusion.5
  210.4 1.3 fusion.157
  213.4 1.3 dynamic_update_slice.19
  217.8 1.3 fusion.157
  220.9 2.7 fusion.49
  223.5 1.7 copy.91
  225.3 1.9 reshape.203
  227.2 1.9 copy.107
  229.9 1.4 fusion.100
  231.4 1.7 fusion.121
  235.6 2.0 fusion.42
  237.7 10.3 %fusion.74 = f32[4,384,3072]{2,1,0:T(8,128)} fusion(bf16[3072,4,128]{0,2,1:T(8,128)(2,1)} %all-gather.7.cloned.1.call-done, bf16[384,4,16]{0,2,1:T(8,128)(2,1)S(1)} %get-tuple-element.274, bf16[384,4,16]{0,2,1:T(8,128)(2,1)S(1)} %get-tuple-element.275), kind=kOutput, calls=%fused_computation.82 | convolution fusion | flops 302186496 | bytes 19759104 | tf_op jit(solution)/shard_map/qhd,khd->hqk/dot_general | solution.py:158
  248.1 17.5 %fusion.14 = (f32[4,384]{1,0:T(4,128)S(1)}, f32[4,384]{1,0:T(4,128)S(1)}, f32[4,384,3072]{2,1,0:T(8,128)}) fusion(pred[384,3072]{1,0:T(8,128)(4,1)S(1)} %copy-done.3, f32[4,384,3072]{2,1,0:T(8,128)} %fusion.74, bf16[3072,4,128]{0,2,1:T(8,128)(2,1)} %all-gather.7.cloned.1.call-done, bf16[384,4,16]{0,2,1:T(8,128)(2,1)S(1)} %get-tuple-element.267, ...), kind=kOutput, calls=%fused_computation.32 | convolution fusion | flops 330494976 | bytes 39825408 | tf_op jit(solution)/shard_map/qhd,khd->hqk/dot_general | solution.py:158
  265.6 17.6 %fusion.17 = (f32[4,384]{1,0:T(4,128)S(1)}, f32[4,384]{1,0:T(4,128)S(1)}) fusion(f32[4,384,3072]{2,1,0:T(8,128)} %get-tuple-element.278, f32[4,384]{1,0:T(4,128)S(1)} %get-tuple-element.285, pred[384,3072]{1,0:T(8,128)(4,1)} %iota_compare_fusion, f32[4,384]{1,0:T(4,128)S(1)} %get-tuple-element.286, f32[4,384,3072]{2,1,0:T(8,128)} %fusion.74), kind=kLoop, calls=%fused_computation.35 | loop fusion | flops 47182848 | bytes 38952960 | tf_op jit(solution)/shard_map/reduce_sum | solution.py:164
  283.5 8.0 %fusion.67 = f32[384,4,64]{0,2,1:T(8,128)S(1)} fusion(bf16[3072,4,128]{0,2,1:T(8,128)(2,1)} %all-gather.7.cloned.1.call-done, f32[4,384,3072]{2,1,0:T(8,128)S(1)} %copy-done.1, f32[4,384]{1,0:T(4,128)S(1)} %get-tuple-element.286, pred[384,3072]{1,0:T(8,128)(4,1)} %iota_compare_fusion, f32[384,4]{0,1:T(4,128)S(1)} %bitcast.239), kind=kOutput, calls=%fused_computation.79 | convolution fusion | flops 627671040 | bytes 22032384 | tf_op jit(solution)/shard_map/hqk,khd->hqd/dot_general | solution.py:165
  291.5 9.9 %multiply_reduce_fusion.1 = (f32[384,4]{0,1:T(4,128)S(1)}, f32[384,4,64]{0,2,1:T(8,128)S(1)}) fusion(f32[384,4,64]{0,2,1:T(8,128)S(1)} %fusion.67, f32[384,4]{0,1:T(4,128)S(1)} %bitcast.238, bf16[3072,4,128]{0,2,1:T(8,128)(2,1)} %all-gather.7.cloned.1.call-done, f32[4,384,3072]{2,1,0:T(8,128)} %get-tuple-element.278, f32[4,384]{1,0:T(4,128)S(1)} %get-tuple-element.285, ...), kind=kOutput, calls=%fused_computation.97 | convolution fusion | flops 628062720 | bytes 22431760 | tf_op jit(solution)/shard_map/hqk,khd->hqd/dot_general | solution.py:165
  302.6 1.8 add_convert_fusion
  304.4 53.7 %reduce-scatter.2.cloned.1.call-done = bf16[384,512]{1,0:T(8,128)(2,1)} async-done(((bf16[384,2048]{1,0:T(8,128)(2,1)}), bf16[384,512]{1,0:T(8,128)(2,1)}) %reduce-scatter.2.cloned.1.call-update) | async-done | bytes 393232 | tf_op jit(solution)/shard_map/reduce_scatter | solution.py:279
  (170 shorter events, 51.6 us)
Async XLA Ops:
  6.5 295.0 %copy-start = (bf16[256,2048]{1,0:T(8,128)(2,1)S(1)}, bf16[256,2048]{1,0:T(8,128)(2,1)}, u32[]{:S(2)}) copy-start(bf16[256,2048]{1,0:T(8,128)(2,1)} %param.34) | copy-start | bytes 3145732
  8.0 6.1 %copy-start.33 = (u32[32]{0:T(128)S(1)}, u32[32]{0:T(128)}, u32[]{:S(2)}) copy-start(u32[32]{0:T(128)} %constant.98) | copy-start | bytes 388
  9.6 25.2 %all-to-all-start = ((bf16[384,4,512]{2,0,1:T(8,128)(2,1)}), bf16[384,4,512]{2,0,1:T(8,128)(2,1)}, u32[]{:S(2)}, u32[]{:S(2)}) async-start(bf16[384,4,512]{2,0,1:T(8,128)(2,1)} %copy.77), calls=%async_computation | async-start | bytes 3145728 | tf_op jit(solution)/shard_map/all_to_all | solution.py:207
  14.0 24.3 %copy-start.24 = (f32[2048]{0:T(1024)S(1)}, f32[2048]{0:T(1024)}, u32[]{:S(2)}) copy-start(f32[2048]{0:T(1024)} %param.21) | copy-start | bytes 24580
  14.0 223.7 %all-gather.7.cloned.1.call-start = ((), (), s32[]{:S(2)}) async-start(), calls=%async_computation.2 | async-start | bytes 3538944 | tf_op jit(solution)/shard_map/all_gather | solution.py:239
  16.2 107.6 %copy-start.7 = (f32[384,16]{0,1:T(8,128)}, f32[384,16]{0,1:T(8,128)S(1)}, u32[]{:S(2)}) copy-start(f32[384,16]{0,1:T(8,128)S(1)} %get-tuple-element.276) | copy-start | bytes 73732
  16.2 107.6 %copy-start.9 = (f32[384,16]{0,1:T(8,128)}, f32[384,16]{0,1:T(8,128)S(1)}, u32[]{:S(2)}) copy-start(f32[384,16]{0,1:T(8,128)S(1)} %get-tuple-element.277) | copy-start | bytes 73732
  36.7 1.2 copy-start.2
  37.9 2.2 copy-start.21
  37.9 2.2 copy-start.25
  37.9 2.2 copy-start.26
  37.9 4.5 %copy-start.22 = (bf16[2048,4]{0,1:T(4,128)(2,1)S(1)}, bf16[2048,4]{0,1:T(4,128)(2,1)}, u32[]{:S(2)}) copy-start(bf16[2048,4]{0,1:T(4,128)(2,1)} %param.28) | copy-start | bytes 49156
  40.1 53.2 %copy-start.19 = (f32[384]{0:T(512)}, f32[384]{0:T(512)S(1)}, u32[]{:S(2)}) copy-start(f32[384]{0:T(512)S(1)} %add_rsqrt_fusion.1) | copy-start | bytes 4612
  42.9 48.9 %copy-start.14 = (f32[6,64,4]{1,0,2:T(8,128)}, f32[6,64,4]{1,0,2:T(8,128)S(1)}, u32[]{:S(2)}) copy-start(f32[6,64,4]{1,0,2:T(8,128)S(1)} %reshape.201) | copy-start | bytes 18436
  84.4 7.4 %copy-start.17 = (f32[4,6,64]{2,1,0:T(8,128)}, f32[4,6,64]{2,1,0:T(8,128)S(1)}, u32[]{:S(2)}) copy-start(f32[4,6,64]{2,1,0:T(8,128)S(1)} %subtract_exponential_fusion.4) | copy-start | bytes 18436
  89.7 2.1 copy-start.28
  91.8 1.5 copy-start.29
  124.8 0.7 copy-start.12
  124.8 8.2 %copy-start.11 = (f32[4,64,64]{2,1,0:T(8,128)S(1)}, f32[4,64,64]{2,1,0:T(8,128)}, u32[]{:S(2)}) copy-start(f32[4,64,64]{2,1,0:T(8,128)} %fusion.83) | copy-start | bytes 196612
  125.5 232.6 %reduce-scatter.2.cloned.1.call-start = ((), (), s32[]{:S(2)}) async-start(), calls=%async_computation.3 | async-start | bytes 1966080 | tf_op jit(solution)/shard_map/reduce_scatter | solution.py:279
  172.6 2.6 copy-start.4
  173.3 2.9 copy-start.16
  220.8 8.3 %copy-start.23 = (f32[6,4]{1,0:T(8,128)S(1)}, f32[6,4]{1,0:T(8,128)}, u32[]{:S(2)}) copy-start(f32[6,4]{1,0:T(8,128)} %get-tuple-element.124) | copy-start | bytes 292
  220.8 8.5 %copy-start.15 = (f32[6,64,4]{1,0,2:T(8,128)S(1)}, f32[6,64,4]{1,0,2:T(8,128)}, u32[]{:S(2)}) copy-start(f32[6,64,4]{1,0,2:T(8,128)} %copy-done.14) | copy-start | bytes 18436
  220.8 8.5 %copy-start.18 = (pred[64,64]{0,1:T(8,128)(4,1)S(1)}, pred[64,64]{0,1:T(8,128)(4,1)}, u32[]{:S(2)}) copy-start(pred[64,64]{0,1:T(8,128)(4,1)} %iota_compare_fusion.1) | copy-start | bytes 12292
  220.9 9.1 %copy-start.31 = (f32[6,4,64]{2,1,0:T(4,128)S(1)}, f32[6,4,64]{2,1,0:T(4,128)}, u32[]{:S(2)}) copy-start(f32[6,4,64]{2,1,0:T(4,128)} %get-tuple-element.126) | copy-start | bytes 18436
  229.3 3.9 %copy-start.5 = (bf16[6,64,4,64]{3,2,1,0:T(4,128)(2,1)S(1)}, bf16[6,64,4,64]{3,2,1,0:T(4,128)(2,1)}, u32[]{:S(2)}) copy-start(bf16[6,64,4,64]{3,2,1,0:T(4,128)(2,1)} %reshape.202) | copy-start | bytes 589828
  229.3 4.7 %copy-start.13 = (bf16[4,6,64,64]{2,3,1,0:T(8,128)(2,1)S(1)}, bf16[4,6,64,64]{2,3,1,0:T(8,128)(2,1)}, u32[]{:S(2)}) copy-start(bf16[4,6,64,64]{2,3,1,0:T(8,128)(2,1)} %copy.107) | copy-start | bytes 589828
  229.3 4.7 %copy-start.30 = (f32[6,4,64,64]{3,2,0,1:T(8,128)S(1)}, f32[6,4,64,64]{3,2,0,1:T(8,128)}, u32[]{:S(2)}) copy-start(f32[6,4,64,64]{3,2,0,1:T(8,128)} %get-tuple-element.125) | copy-start | bytes 1179652
  233.2 2.4 copy-start.20
  235.0 2.7 copy-start.8
  235.0 2.7 copy-start.10
  237.7 10.4 %copy-start.3 = (pred[384,3072]{1,0:T(8,128)(4,1)S(1)}, pred[384,3072]{1,0:T(8,128)(4,1)}, u32[]{:S(2)}) copy-start(pred[384,3072]{1,0:T(8,128)(4,1)} %iota_compare_fusion) | copy-start | bytes 3538948
  265.6 17.9 %copy-start.1 = (f32[4,384,3072]{2,1,0:T(8,128)S(1)}, f32[4,384,3072]{2,1,0:T(8,128)}, u32[]{:S(2)}) copy-start(f32[4,384,3072]{2,1,0:T(8,128)} %fusion.74) | copy-start | bytes 56623108
  283.5 8.0 %copy-start.32 = (f32[4]{0:T(128)S(1)}, f32[4]{0:T(128)}, u32[]{:S(2)}) copy-start(f32[4]{0:T(128)} %param.32) | copy-start | bytes 52
  291.5 9.9 %copy-start.27 = (f32[64]{0:T(128)S(1)}, f32[64]{0:T(128)}, u32[]{:S(2)}) copy-start(f32[64]{0:T(128)} %param.33) | copy-start | bytes 772
  301.4 1.2 copy-start.6
Sparse Core Ops, SparseCore 0:
  125.7 67.2 all-gather.6
  304.6 53.5 reduce-scatter.1
